TPU v7x, 256 devices: a 4x2x16 block of a 4x16x16 slice. The times are simulated.
256 devices in a mesh: grp: 2 (over y), fs: 16 (over z), tp: 8 (over x, core).
Axes of the slice: x: 4, y: 2, z: 16, core: 2. Of those that a mesh axis runs over, the one named last changes fastest.
The devices are a block of a 4x16x16 slice.
Arguments:
- layer_input: bfloat16 [12288, 2048], P(('grp', 'fs'), 'tp'), parts along dimension 0, may hold values from -6 to 6
- first_gain: bfloat16 [1, 2048], P(None, 'tp'), may hold values from 0.099609375 to 1.8984375
- ffn_gate_w: bfloat16 [2048, 6144], P('fs', 'tp'), may hold values from -0.125 to 0.125
- ffn_up_w: bfloat16 [2048, 6144], P('fs', 'tp'), may hold values from -0.125 to 0.125
- ffn_down_w: bfloat16 [6144, 2048], P('tp', 'fs'), may hold values from -0.078125 to 0.078125
- mixer_gain: bfloat16 [1, 2048], P(None, 'tp'), may hold values from 0.099609375 to 1.8984375
- pool_in_w: bfloat16 [2048, 1024], P('fs', 'tp'), may hold values from -0.125 to 0.125
- mixer_gate_w: bfloat16 [2048, 2048], P('fs', 'tp'), may hold values from -0.125 to 0.125
- group_mix_w: bfloat16 [8, 128, 128], P('tp'), may hold values from -0.5 to 0.5
- pool_scale: float32 [1, 1024], P(None, 'tp'), may hold values from 0.1 to 1.9
- mixer_out_w: bfloat16 [1024, 2048], P('tp', 'fs'), may hold values from -0.1875 to 0.1875
- second_gain: bfloat16 [1, 2048], P(None, 'tp'), may hold values from 0.099609375 to 1.8984375
Outputs:
- layer_output: bfloat16 [12288, 2048], P(('grp', 'fs'), 'tp'), parts along dimension 0
There are 2 independent parts, one for each index of `grp`. A program takes and returns all parts, laid end to end along the dimension named above; an argument that names none is the same for every part. Nothing has to cross between parts.
All inputs are finite; a program needn't handle non-finite values.
Results may differ from a plain program's by a relative error of at most 0.015.
Values may be sent and summed in bfloat16 or wider, within the bound.
A program may use at most 64 MiB of HBM per device.

v0:
```python
import jax
import jax.numpy as jnp
from jax import lax
from jax.sharding import Mesh
from jax.sharding import PartitionSpec as P

TP = ("tp_0", "tp_1")


def from_everyone(value, axis):
    length = lax.axis_size(axis)
    return lax.all_to_all(
        jnp.broadcast_to(value[None], (length, *value.shape)), axis, 0, 0, tiled=True
    )


def joined_along(tiles, dim):
    shape = list(tiles.shape[1:])
    shape[dim] *= tiles.shape[0]
    return jnp.moveaxis(tiles, 0, dim).reshape(shape)


def whole_of(value, axes, dim):
    far, near = axes
    initial = from_everyone(value, far)
    tiles = jnp.swapaxes(from_everyone(initial, near), 0, 1)
    return joined_along(tiles.reshape(-1, *value.shape), dim)


def in_one_piece(arrays, axis, dim, along):
    widths = [a.shape[along] for a in arrays]
    both = jnp.concatenate(arrays, axis=along)
    filled = whole_of(both, axis, dim)
    return tuple(jnp.split(filled, [sum(widths[:k]) for k in range(1, len(widths))], axis=along))


def in_blocks(value, dim, length):
    before, after = (value.shape[:dim], value.shape[dim + 1 :])
    return jnp.moveaxis(value.reshape(*before, length, -1, *after), dim, 0)


def summed_on_arrival(value, axis, dim):
    tiles = in_blocks(value, dim, lax.axis_size(axis))
    arrived = lax.all_to_all(tiles, axis, split_axis=0, concat_axis=0, tiled=True)
    return arrived.astype(jnp.float32).sum(axis=0)


def sent_together(arrays, axis, dim, along):
    ends, at = ([], 0)
    for a in arrays[:-1]:
        at += a.shape[along]
        ends.append(at)
    both = jnp.concatenate(arrays, axis=along)
    return tuple(jnp.split(lax.all_gather(both, axis, axis=dim, tiled=True), ends, axis=along))


def gather_directly(value, axis, dim):
    return joined_along(from_everyone(value, axis), dim)


def norm_rows(values, gain):
    gathered, gain_whole = in_one_piece((values, gain), ("tp_0", "tp_1"), 1, 0)
    widened = gathered.astype(jnp.float32)
    scaled = (widened * gain_whole.astype(jnp.float32)).astype(jnp.bfloat16)
    factor = lax.rsqrt(jnp.mean(widened * widened, axis=1, keepdims=True) + 1e-06)
    return (scaled, factor)


def column_sums(partial_value):
    return summed_on_arrival(partial_value.astype(jnp.bfloat16), TP, 1)


def add_pair(scaled, pieces):
    first_sum = jnp.dot(scaled, pieces[0], preferred_element_type=jnp.float32)
    second_sum = jnp.dot(scaled, pieces[1], preferred_element_type=jnp.float32)
    return (first_sum, second_sum)


def per_device(
    layer_input,
    first_gain,
    ffn_gate_w,
    ffn_up_w,
    ffn_down_w,
    mixer_gain,
    pool_in_w,
    mixer_gate_w,
    group_mix_w,
    pool_scale,
    mixer_out_w,
    second_gain,
):
    row_count = layer_input.shape[0]
    gate_whole, up_whole = sent_together((ffn_gate_w, ffn_up_w), "fs", 0, 1)
    down_whole = lax.all_gather(ffn_down_w, "fs", axis=1, tiled=True)

    def feed_forward(values, gain):
        scaled, factor = norm_rows(values, gain)
        gate_pre = factor * jnp.dot(scaled, gate_whole, preferred_element_type=jnp.float32)
        up_pre = factor * jnp.dot(scaled, up_whole, preferred_element_type=jnp.float32)
        hidden = (jax.nn.silu(gate_pre) * up_pre).astype(jnp.bfloat16)
        return jnp.dot(hidden, down_whole, preferred_element_type=jnp.float32)

    first = (
        layer_input.astype(jnp.float32) + 0.5 * column_sums(feed_forward(layer_input, first_gain))
    ).astype(jnp.bfloat16)
    scaled, factor = norm_rows(first, mixer_gain)
    pool_sum, gate_sum = add_pair(scaled, sent_together((pool_in_w, mixer_gate_w), "fs", 0, 1))
    pool_pre = (factor * pool_sum).astype(jnp.bfloat16)
    gate_logit = factor * gate_sum
    group_count = group_mix_w.shape[0]
    group_width = group_mix_w.shape[1]
    first_group = lax.axis_index(TP) * group_count
    values = pool_pre.astype(jnp.float32).reshape(row_count, group_count, group_width)
    running = jnp.cumsum(values, axis=0)
    positions = jnp.arange(row_count, dtype=jnp.int32)
    windows = 2 ** (1 + (first_group + jnp.arange(group_count, dtype=jnp.int32)) % 4)
    chosen = jnp.zeros_like(values)
    for span in (2, 4, 8, 16):
        lagged = jnp.pad(running, ((span, 0), (0, 0), (0, 0)))[:row_count]
        counts = jnp.minimum(positions + 1, span).astype(jnp.float32)[:, None, None]
        means = (running - lagged) / counts
        chosen = jnp.where((windows == span)[None, :, None], means, chosen)
    trail = (chosen - values).astype(jnp.bfloat16)
    mixed = jnp.einsum("tgc,gcd->tgd", trail, group_mix_w, preferred_element_type=jnp.float32)
    pooled = (mixed.reshape(row_count, group_count * group_width) * pool_scale).astype(jnp.bfloat16)
    lifted = column_sums(
        jnp.dot(pooled, gather_directly(mixer_out_w, "fs", 1), preferred_element_type=jnp.float32)
    )
    second = (first.astype(jnp.float32) + jax.nn.sigmoid(gate_logit) * lifted).astype(jnp.bfloat16)
    result = second.astype(jnp.float32) + 0.5 * column_sums(feed_forward(second, second_gain))
    return result.astype(jnp.bfloat16)


def solution(mesh):
    finer = Mesh(
        mesh.devices.reshape(mesh.shape["grp"], mesh.shape["fs"], 4, 2),
        ("grp", "fs", "tp_0", "tp_1"),
    )
    return jax.shard_map(
        per_device,
        mesh=finer,
        in_specs=(
            P(("grp", "fs"), TP),
            P(None, TP),
            P("fs", TP),
            P("fs", TP),
            P(TP, "fs"),
            P(None, TP),
            P("fs", TP),
            P("fs", TP),
            P(TP, None, None),
            P(None, TP),
            P(TP, "fs"),
            P(None, TP),
        ),
        out_specs=P(("grp", "fs"), TP),
        check_vma=False,
    )
```

profile of v0, /device:TPU:33, one launch (start us, length us, event | category | flops | bytes accessed | tf_op | source)
XLA Modules:
  0.0 387.3 jit_solution(81376959434211735)
XLA Ops:
  10.3 13.3 %all_to_all.50 = bf16[4,385,256]{2,1,0:T(8,128)(2,1)S(1)} all-to-all(bf16[4,385,256]{2,1,0:T(8,128)(2,1)S(1)} %broadcast_in_dim.91), channel_id=1, replica_groups=mesh['grp'=2,'fs'=16,'tp_0'=4,'tp_1'=2] {'tp_0'}, dimensions={0} | all-to-all | bytes 1576960 | tf_op jit(solution)/shard_map/all_to_all | solution.py:12
  24.3 23.7 %all_to_all.51 = bf16[2,4,385,256]{3,1,2,0:T(4,128)(2,1)S(1)} all-to-all(bf16[2,4,385,256]{3,1,2,0:T(4,128)(2,1)S(1)} %broadcast_in_dim.92), channel_id=1, replica_groups=mesh['grp'=2,'fs'=16,'tp_0'=4,'tp_1'=2] {'tp_1'}, dimensions={0} | all-to-all | bytes 3153920 | tf_op jit(solution)/shard_map/all_to_all | solution.py:12
  50.2 3.6 copy.35
  56.4 48.7 %all-gather.4.cloned.1.call-done = bf16[2048,1536]{1,0:T(8,128)(2,1)} async-done(((bf16[128,1536]{1,0:T(8,128)(2,1)}), bf16[2048,1536]{1,0:T(8,128)(2,1)}) %all-gather.4.cloned.1.call-update) | async-done | bytes 6291472 | tf_op jit(solution)/shard_map/all_gather | solution.py:54
  105.1 4.3 %fusion.11 = f32[384,768]{1,0:T(8,128)} fusion(bf16[384,2048]{0,1:T(8,128)(2,1)S(1)} %fusion.2, bf16[2048,1536]{1,0:T(8,128)(2,1)} %all-gather.4.cloned.1.call-done, f32[384]{0:T(512)S(1)} %add_rsqrt_fusion.2), kind=kOutput, calls=%fused_computation.29 | convolution fusion | flops 1208254464 | bytes 5899776 | tf_op jit(solution)/shard_map/dot_general | solution.py:99
  109.4 71.1 %all-gather.6.cloned.1.call-done = bf16[768,2048]{1,0:T(8,128)(2,1)} async-done(((bf16[768,128]{1,0:T(8,128)(2,1)}), bf16[768,2048]{1,0:T(8,128)(2,1)}) %all-gather.6.cloned.1.call-update) | async-done | bytes 3145744 | tf_op jit(solution)/shard_map/all_gather | solution.py:95
  180.5 6.4 %convolution_convert_fusion.1 = bf16[384,2048]{1,0:T(8,128)(2,1)S(1)} fusion(bf16[768,2048]{1,0:T(8,128)(2,1)} %all-gather.6.cloned.1.call-done, bf16[384,2048]{0,1:T(8,128)(2,1)S(1)} %fusion.2, bf16[2048,1536]{1,0:T(8,128)(2,1)} %all-gather.4.cloned.1.call-done, f32[384,768]{1,0:T(8,128)} %fusion.11, f32[384]{0:T(512)S(1)} %add_rsqrt_fusion.2), kind=kOutput, calls=%fused_computation.13 | convolution fusion | flops 2418769920 | bytes 10618368 | tf_op jit(solution)/shard_map/dot_general | solution.py:102
  188.1 15.3 %all-to-all-start.2 = ((bf16[8,384,256]{2,1,0:T(8,128)(2,1)}), bf16[8,384,256]{2,1,0:T(8,128)(2,1)S(1)}, u32[]{:S(2)}, u32[]{:S(2)}) async-start(bf16[8,384,256]{2,1,0:T(8,128)(2,1)} %bitcast.111), calls=%async_computation.2 | async-start | bytes 3145728 | tf_op jit(solution)/shard_map/all_to_all | solution.py:44
  204.2 19.8 %all-to-all-done.2 = bf16[8,384,256]{2,1,0:T(8,128)(2,1)S(1)} async-done(((bf16[8,384,256]{2,1,0:T(8,128)(2,1)}), bf16[8,384,256]{2,1,0:T(8,128)(2,1)S(1)}, u32[]{:S(2)}, u32[]{:S(2)}) %all-to-all-start.2) | async-done | bytes 1572896 | tf_op jit(solution)/shard_map/all_to_all | solution.py:44
  225.3 3.6 all-to-all-start.3
  229.1 11.3 %all-to-all-done.3 = bf16[4,385,256]{2,1,0:T(8,128)(2,1)S(1)} async-done(((bf16[4,385,256]{2,1,0:T(8,128)(2,1)}), bf16[4,385,256]{2,1,0:T(8,128)(2,1)S(1)}, u32[]{:S(2)}, u32[]{:S(2)}) %all-to-all-start.3) | async-done | bytes 788512 | tf_op jit(solution)/shard_map/all_to_all | solution.py:12
  241.1 6.5 %all_to_all.52 = bf16[2,4,385,256]{3,1,2,0:T(4,128)(2,1)S(1)} all-to-all(bf16[2,4,385,256]{3,1,2,0:T(4,128)(2,1)S(1)} %broadcast_in_dim.94), channel_id=1, replica_groups=mesh['grp'=2,'fs'=16,'tp_0'=4,'tp_1'=2] {'tp_1'}, dimensions={0} | all-to-all | bytes 3153920 | tf_op jit(solution)/shard_map/all_to_all | solution.py:12
  248.5 7.0 %all-to-all-start.5 = ((bf16[16,128,128]{1,2,0:T(8,128)(2,1)}), bf16[16,128,128]{1,2,0:T(8,128)(2,1)}, u32[]{:S(2)}, u32[]{:S(2)}) async-start(bf16[16,128,128]{1,2,0:T(8,128)(2,1)} %broadcast_in_dim.104), calls=%async_computation.5 | async-start | bytes 1048576 | tf_op jit(solution)/shard_map/all_to_all | solution.py:12
  257.6 3.5 copy.39
  263.8 3.6 all-gather.8.cloned.1.call-done
  270.7 10.8 %all-to-all-done.5 = bf16[16,128,128]{1,2,0:T(8,128)(2,1)} async-done(((bf16[16,128,128]{1,2,0:T(8,128)(2,1)}), bf16[16,128,128]{1,2,0:T(8,128)(2,1)}, u32[]{:S(2)}, u32[]{:S(2)}) %all-to-all-start.5) | async-done | bytes 524320 | tf_op jit(solution)/shard_map/all_to_all | solution.py:12
  281.5 2.4 convolution_convert_fusion.2
  284.0 31.3 %all_to_all.53 = bf16[8,384,256]{2,1,0:T(8,128)(2,1)S(1)} all-to-all(bf16[8,384,256]{2,1,0:T(8,128)(2,1)S(1)} %bitcast.125), channel_id=1, replica_groups=mesh['grp'=2,'fs'=16,'tp_0'=4,'tp_1'=2] {'tp_0','tp_1'}, dimensions={0} | all-to-all | bytes 3145728 | tf_op jit(solution)/shard_map/all_to_all | solution.py:44
  318.1 13.9 %all_to_all.54 = bf16[4,385,256]{2,1,0:T(8,128)(2,1)S(1)} all-to-all(bf16[4,385,256]{2,1,0:T(8,128)(2,1)S(1)} %broadcast_in_dim.105), channel_id=1, replica_groups=mesh['grp'=2,'fs'=16,'tp_0'=4,'tp_1'=2] {'tp_0'}, dimensions={0} | all-to-all | bytes 1576960 | tf_op jit(solution)/shard_map/all_to_all | solution.py:12
  332.7 6.5 %all_to_all.55 = bf16[2,4,385,256]{3,1,2,0:T(4,128)(2,1)S(1)} all-to-all(bf16[2,4,385,256]{3,1,2,0:T(4,128)(2,1)S(1)} %broadcast_in_dim.106), channel_id=1, replica_groups=mesh['grp'=2,'fs'=16,'tp_0'=4,'tp_1'=2] {'tp_1'}, dimensions={0} | all-to-all | bytes 3153920 | tf_op jit(solution)/shard_map/all_to_all | solution.py:12
  341.8 2.4 copy.46
  345.7 3.3 fusion.14
  349.1 6.5 %convolution_convert_fusion = bf16[384,2048]{1,0:T(8,128)(2,1)S(1)} fusion(bf16[768,2048]{1,0:T(8,128)(2,1)} %all-gather.6.cloned.1.call-done, bf16[384,2048]{0,1:T(8,128)(2,1)} %copy-done.2, bf16[2048,1536]{1,0:T(8,128)(2,1)} %all-gather.4.cloned.1.call-done, f32[384,768]{1,0:T(8,128)S(1)} %fusion.14, f32[384]{0:T(512)S(1)} %add_rsqrt_fusion), kind=kOutput, calls=%fused_computation.12 | convolution fusion | flops 2418769920 | bytes 10618368 | tf_op jit(solution)/shard_map/dot_general | solution.py:102
  355.7 23.4 %all_to_all.56 = bf16[8,384,256]{2,1,0:T(8,128)(2,1)S(1)} all-to-all(bf16[8,384,256]{2,1,0:T(8,128)(2,1)S(1)} %bitcast.126), channel_id=1, replica_groups=mesh['grp'=2,'fs'=16,'tp_0'=4,'tp_1'=2] {'tp_0','tp_1'}, dimensions={0} | all-to-all | bytes 3145728 | tf_op jit(solution)/shard_map/all_to_all | solution.py:44
  (87 shorter events, 31.6 us)
Async XLA Ops:
  6.5 275.0 %copy-start = (bf16[1,128,128]{2,1,0:T(8,128)(2,1)S(1)}, bf16[1,128,128]{2,1,0:T(8,128)(2,1)}, u32[]{:S(2)}) copy-start(bf16[1,128,128]{2,1,0:T(8,128)(2,1)} %param.20) | copy-start | bytes 98308
  6.6 98.6 %all-gather.4.cloned.1.call-start = ((), (), s32[]{:S(2)}) async-start(), calls=%async_computation.10 | async-start | bytes 6684672 | tf_op jit(solution)/shard_map/all_gather | solution.py:54
  8.4 172.1 %all-gather.6.cloned.1.call-start = ((), (), s32[]{:S(2)}) async-start(), calls=%async_computation.11 | async-start | bytes 3342336 | tf_op jit(solution)/shard_map/all_gather | solution.py:95
  188.1 15.4 %copy-start.7 = (bf16[128,256]{1,0:T(8,128)(2,1)S(1)}, bf16[128,256]{1,0:T(8,128)(2,1)}, u32[]{:S(2)}) copy-start(bf16[128,256]{1,0:T(8,128)(2,1)} %param.19) | copy-start | bytes 196612
  188.1 15.4 %copy-start.9 = (bf16[128,128]{1,0:T(8,128)(2,1)S(1)}, bf16[128,128]{1,0:T(8,128)(2,1)}, u32[]{:S(2)}) copy-start(bf16[128,128]{1,0:T(8,128)(2,1)} %param.18) | copy-start | bytes 98308
  188.1 35.9 %all-to-all-start.2 = ((bf16[8,384,256]{2,1,0:T(8,128)(2,1)}), bf16[8,384,256]{2,1,0:T(8,128)(2,1)S(1)}, u32[]{:S(2)}, u32[]{:S(2)}) async-start(bf16[8,384,256]{2,1,0:T(8,128)(2,1)} %bitcast.111), calls=%async_computation.2 | async-start | bytes 3145728 | tf_op jit(solution)/shard_map/all_to_all | solution.py:44
  203.4 20.8 %copy-start.3 = (bf16[384,256]{1,0:T(8,128)(2,1)S(1)}, bf16[384,256]{1,0:T(8,128)(2,1)}, u32[]{:S(2)}) copy-start(bf16[384,256]{1,0:T(8,128)(2,1)} %param.12) | copy-start | bytes 589828
  203.4 20.9 %copy-start.10 = (bf16[1,256]{1,0:T(2,128)(2,1)S(1)}, bf16[1,256]{1,0:T(2,128)(2,1)}, u32[]{:S(2)}) copy-start(bf16[1,256]{1,0:T(2,128)(2,1)} %param.17) | copy-start | bytes 1540
  203.4 64.0 %all-gather.8.cloned.1.call-start = ((), (), s32[]{:S(2)}) async-start(), calls=%async_computation.12 | async-start | bytes 1671168 | tf_op jit(solution)/shard_map/all_gather | solution.py:54
  224.3 4.6 %copy-start.8 = (bf16[128,128]{1,0:T(8,128)(2,1)S(1)}, bf16[128,128]{1,0:T(8,128)(2,1)}, u32[]{:S(2)}) copy-start(bf16[128,128]{1,0:T(8,128)(2,1)} %param.22) | copy-start | bytes 98308
  225.3 15.1 %all-to-all-start.3 = ((bf16[4,385,256]{2,1,0:T(8,128)(2,1)}), bf16[4,385,256]{2,1,0:T(8,128)(2,1)S(1)}, u32[]{:S(2)}, u32[]{:S(2)}) async-start(bf16[4,385,256]{2,1,0:T(8,128)(2,1)} %broadcast_in_dim.93), calls=%async_computation.3 | async-start | bytes 1605632 | tf_op jit(solution)/shard_map/all_to_all | solution.py:12
  248.5 33.0 %all-to-all-start.5 = ((bf16[16,128,128]{1,2,0:T(8,128)(2,1)}), bf16[16,128,128]{1,2,0:T(8,128)(2,1)}, u32[]{:S(2)}, u32[]{:S(2)}) async-start(bf16[16,128,128]{1,2,0:T(8,128)(2,1)} %broadcast_in_dim.104), calls=%async_computation.5 | async-start | bytes 1048576 | tf_op jit(solution)/shard_map/all_to_all | solution.py:12
  269.1 0.7 copy-start.6
  269.1 12.4 %copy-start.13 = (f32[1,128]{1,0:T(1,128)S(1)}, f32[1,128]{1,0:T(1,128)}, u32[]{:S(2)}) copy-start(f32[1,128]{1,0:T(1,128)} %param.21) | copy-start | bytes 1540
  315.3 1.4 copy-start.12
  316.7 0.7 copy-start.11
  317.4 0.7 copy-start.4
  344.6 1.2 copy-start.2
  355.7 25.1 %copy-start.1 = (bf16[1,128,128]{2,1,0:T(8,128)(2,1)S(1)}, bf16[1,128,128]{2,1,0:T(8,128)(2,1)}, u32[]{:S(2)}) copy-start(bf16[1,128,128]{2,1,0:T(8,128)(2,1)} %param.20) | copy-start | bytes 98308
  379.1 0.9 copy-start.5
Sparse Core Ops, SparseCore 0:
  9.1 95.9 all-gather.3
  106.8 73.5 all-gather.5
  206.1 61.3 all-gather.7
where the time goes:
time: 388 us; the launch traced here: 387 us
  waiting for transfers between devices  166 us (43%)
  blocking collectives  119 us (31%)
  starting transfers between devices  26 us (7%)
  matrix products  25.2 us (6%)
  local copies, waits for them, and re-layouts  20.2 us (5%)
  other arithmetic  17.6 us (5%)
  between operations  13.6 us (4%)
    all_gather x1, waiting for transfers between devices, per_device(): down_whole = lax.all_gather(ffn_down_w, 'fs', axis=1, tiled=True)  71.1 us
    all_to_all x5, blocking collectives, from_everyone(): lax.all_to_all(jnp.broadcast_to(value[None], (length, *value.shape)), axi...  64 us
    all_to_all x2, blocking collectives, summed_on_arrival(): lax.all_to_all(tiles, axis, split_axis=0, concat_axis=0, tiled=True)  54.7 us
    all_gather x2, waiting for transfers between devices, sent_together(): lax.all_gather(both, axis, axis=dim, tiled=True)  52.3 us
    all_to_all x2, waiting for transfers between devices, from_everyone(): lax.all_to_all(jnp.broadcast_to(value[None], (length, *value.shape)), axi...  22.1 us
    all_to_all x1, waiting for transfers between devices, summed_on_arrival(): lax.all_to_all(tiles, axis, split_axis=0, concat_axis=0, tiled=True)  19.8 us
    all_to_all x1, starting transfers between devices, summed_on_arrival(): lax.all_to_all(tiles, axis, split_axis=0, concat_axis=0, tiled=True)  15.3 us
    dot_general x2, matrix products, feed_forward(): return jnp.dot(hidden, down_whole, preferred_element_type=jnp.float32)  12.9 us
  transfers between devices with their start and end apart: 6, of which 6 were waited for; matrix products, arithmetic and copies ran while one was open for 7% of the time, Pallas kernels for 0%

commit v1 on v0

--- a/solution.py
+++ b/solution.py
@@ -92,7 +92,9 @@
 ):
     row_count = layer_input.shape[0]
     gate_whole, up_whole = sent_together((ffn_gate_w, ffn_up_w), "fs", 0, 1)
-    down_whole = lax.all_gather(ffn_down_w, "fs", axis=1, tiled=True)
+    down_whole = jnp.concatenate(
+        lax.all_to_all(jnp.stack([ffn_down_w] * lax.axis_size("fs")), "fs", 0, 0), axis=1
+    )
 
     def feed_forward(values, gain):
         scaled, factor = norm_rows(values, gain)

time: 388 us -> 452 us (1.16)
  waiting for transfers between devices: 166 us -> 234 us
  blocking collectives: 119 us -> 105 us
  starting transfers between devices: 26 us -> 33.2 us
    all_gather x2, waiting for transfers between devices: 52.3 us -> 184 us  [sent_together(): lax.all_gather(both, axis, axis=dim, tiled=True)]
    all_gather x1 -> x0, waiting for transfers between devices: 71.1 us -> none  [per_device(): down_whole = lax.all_gather(ffn_down_w, 'fs', axis=1, tiled=True)]
    all_to_all x5 -> x4, blocking collectives: 64 us -> 51.5 us  [from_everyone(): lax.all_to_all(jnp.broadcast_to(value[None], (length, *value.shape)), axi...]
    all_to_all x0 -> x1, starting transfers between devices: none -> 8.75 us  [per_device(): lax.all_to_all(jnp.stack([ffn_down_w] * lax.axis_size('fs')), 'fs', 0, 0)]
    all_to_all x1, starting transfers between devices: 15.3 us -> 7.76 us  [summed_on_arrival(): lax.all_to_all(tiles, axis, split_axis=0, concat_axis=0, tiled=True)]
    all_to_all x2 -> x3, waiting for transfers between devices: 22.1 us -> 29.6 us  [from_everyone(): lax.all_to_all(jnp.broadcast_to(value[None], (length, *value.shape)), axi...]
    all_to_all x2 -> x3, starting transfers between devices: 10.5 us -> 16.7 us  [from_everyone(): lax.all_to_all(jnp.broadcast_to(value[None], (length, *value.shape)), axi...]
  transfers between devices with their start and end apart: 6 -> 7, of which waited for: 6 -> 6; matrix products, arithmetic and copies ran while one was open for 7% -> 7% of each run, Pallas kernels for 0% -> 0%
where the time goes in v1:
time: 452 us; the launch traced here: 451 us
  waiting for transfers between devices  234 us (52%)
  blocking collectives  105 us (23%)
  starting transfers between devices  33.2 us (7%)
  matrix products  25.3 us (6%)
  local copies, waits for them, and re-layouts  23.2 us (5%)
  other arithmetic  16.6 us (4%)
  between operations  13.9 us (3%)
    all_gather x2, waiting for transfers between devices, sent_together(): lax.all_gather(both, axis, axis=dim, tiled=True)  184 us
    all_to_all x2, blocking collectives, summed_on_arrival(): lax.all_to_all(tiles, axis, split_axis=0, concat_axis=0, tiled=True)  53.9 us
    all_to_all x4, blocking collectives, from_everyone(): lax.all_to_all(jnp.broadcast_to(value[None], (length, *value.shape)), axi...  51.5 us
    all_to_all x3, waiting for transfers between devices, from_everyone(): lax.all_to_all(jnp.broadcast_to(value[None], (length, *value.shape)), axi...  29.6 us
    all_to_all x1, waiting for transfers between devices, summed_on_arrival(): lax.all_to_all(tiles, axis, split_axis=0, concat_axis=0, tiled=True)  19.8 us
    all_to_all x3, starting transfers between devices, from_everyone(): lax.all_to_all(jnp.broadcast_to(value[None], (length, *value.shape)), axi...  16.7 us
    dot_general x2, matrix products, feed_forward(): return jnp.dot(hidden, down_whole, preferred_element_type=jnp.float32)  12.9 us
    convert_element_type x3, local copies, waits for them, and re-layouts, norm_rows(): widened = gathered.astype(jnp.float32)  9.45 us
  transfers between devices with their start and end apart: 7, of which 6 were waited for; matrix products, arithmetic and copies ran while one was open for 7% of the time, Pallas kernels for 0%

profile of v1, /device:TPU:33, one launch (start us, length us, event | category | flops | bytes accessed | tf_op | source)
XLA Modules:
  0.0 451.2 jit_solution(1848715493392555394)
XLA Ops:
  8.5 5.2 %all-to-all-start = ((bf16[4,385,256]{2,1,0:T(8,128)(2,1)}), bf16[4,385,256]{2,1,0:T(8,128)(2,1)S(1)}, u32[]{:S(2)}, u32[]{:S(2)}) async-start(bf16[4,385,256]{2,1,0:T(8,128)(2,1)} %broadcast_in_dim.91), calls=%async_computation | async-start | bytes 1605632 | tf_op jit(solution)/shard_map/all_to_all | solution.py:12
  14.8 7.4 %all-to-all-done = bf16[4,385,256]{2,1,0:T(8,128)(2,1)S(1)} async-done(((bf16[4,385,256]{2,1,0:T(8,128)(2,1)}), bf16[4,385,256]{2,1,0:T(8,128)(2,1)S(1)}, u32[]{:S(2)}, u32[]{:S(2)}) %all-to-all-start) | async-done | bytes 788512 | tf_op jit(solution)/shard_map/all_to_all | solution.py:12
  22.9 24.6 %all_to_all.55 = bf16[2,4,385,256]{3,1,2,0:T(4,128)(2,1)S(1)} all-to-all(bf16[2,4,385,256]{3,1,2,0:T(4,128)(2,1)S(1)} %broadcast_in_dim.92), channel_id=1, replica_groups=mesh['grp'=2,'fs'=16,'tp_0'=4,'tp_1'=2] {'tp_1'}, dimensions={0} | all-to-all | bytes 3153920 | tf_op jit(solution)/shard_map/all_to_all | solution.py:12
  49.5 8.8 %all-to-all-start.2 = ((bf16[16,768,128]{1,2,0:T(8,128)(2,1)}), bf16[16,768,128]{1,2,0:T(8,128)(2,1)}, u32[]{:S(2)}, u32[]{:S(2)}) async-start(bf16[16,768,128]{1,2,0:T(8,128)(2,1)} %stack.2), calls=%async_computation.2 | async-start | bytes 6291456 | tf_op jit(solution)/shard_map/all_to_all | solution.py:96
  60.4 3.6 copy.37
  66.6 180.5 %all-gather.3.cloned.1.call-done = bf16[2048,1536]{1,0:T(8,128)(2,1)} async-done(((bf16[128,1536]{1,0:T(8,128)(2,1)}), bf16[2048,1536]{1,0:T(8,128)(2,1)}) %all-gather.3.cloned.1.call-update) | async-done | bytes 6291472 | tf_op jit(solution)/shard_map/all_gather | solution.py:54
  247.1 4.4 fusion.11
  251.5 6.4 %convolution_convert_fusion.1 = bf16[384,2048]{1,0:T(8,128)(2,1)S(1)} fusion(bf16[768,2048]{0,1:T(8,128)(2,1)} %bitcast.7, bf16[384,2048]{0,1:T(8,128)(2,1)S(1)} %fusion.2, bf16[2048,1536]{1,0:T(8,128)(2,1)} %all-gather.3.cloned.1.call-done, f32[384,768]{1,0:T(8,128)} %fusion.11, f32[384]{0:T(512)S(1)} %add_rsqrt_fusion.2), kind=kOutput, calls=%fused_computation.13 | convolution fusion | flops 2418769920 | bytes 10618368 | tf_op jit(solution)/shard_map/dot_general | solution.py:104
  259.1 7.8 %all-to-all-start.3 = ((bf16[8,384,256]{2,1,0:T(8,128)(2,1)}), bf16[8,384,256]{2,1,0:T(8,128)(2,1)S(1)}, u32[]{:S(2)}, u32[]{:S(2)}) async-start(bf16[8,384,256]{2,1,0:T(8,128)(2,1)} %bitcast.114), calls=%async_computation.3 | async-start | bytes 3145728 | tf_op jit(solution)/shard_map/all_to_all | solution.py:44
  267.7 19.8 %all-to-all-done.3 = bf16[8,384,256]{2,1,0:T(8,128)(2,1)S(1)} async-done(((bf16[8,384,256]{2,1,0:T(8,128)(2,1)}), bf16[8,384,256]{2,1,0:T(8,128)(2,1)S(1)}, u32[]{:S(2)}, u32[]{:S(2)}) %all-to-all-start.3) | async-done | bytes 1572896 | tf_op jit(solution)/shard_map/all_to_all | solution.py:44
  288.7 3.6 all-to-all-start.4
  292.5 11.3 %all-to-all-done.4 = bf16[4,385,256]{2,1,0:T(8,128)(2,1)S(1)} async-done(((bf16[4,385,256]{2,1,0:T(8,128)(2,1)}), bf16[4,385,256]{2,1,0:T(8,128)(2,1)S(1)}, u32[]{:S(2)}, u32[]{:S(2)}) %all-to-all-start.4) | async-done | bytes 788512 | tf_op jit(solution)/shard_map/all_to_all | solution.py:12
  304.6 6.5 %all_to_all.56 = bf16[2,4,385,256]{3,1,2,0:T(4,128)(2,1)S(1)} all-to-all(bf16[2,4,385,256]{3,1,2,0:T(4,128)(2,1)S(1)} %broadcast_in_dim.94), channel_id=1, replica_groups=mesh['grp'=2,'fs'=16,'tp_0'=4,'tp_1'=2] {'tp_1'}, dimensions={0} | all-to-all | bytes 3153920 | tf_op jit(solution)/shard_map/all_to_all | solution.py:12
  312.0 7.8 %all-to-all-start.6 = ((bf16[16,128,128]{1,2,0:T(8,128)(2,1)}), bf16[16,128,128]{1,2,0:T(8,128)(2,1)}, u32[]{:S(2)}, u32[]{:S(2)}) async-start(bf16[16,128,128]{1,2,0:T(8,128)(2,1)} %broadcast_in_dim.104), calls=%async_computation.6 | async-start | bytes 1048576 | tf_op jit(solution)/shard_map/all_to_all | solution.py:12
  321.9 3.5 copy.42
  328.1 3.6 all-gather.5.cloned.1.call-done
  335.0 10.9 %all-to-all-done.6 = bf16[16,128,128]{1,2,0:T(8,128)(2,1)} async-done(((bf16[16,128,128]{1,2,0:T(8,128)(2,1)}), bf16[16,128,128]{1,2,0:T(8,128)(2,1)}, u32[]{:S(2)}, u32[]{:S(2)}) %all-to-all-start.6) | async-done | bytes 524320 | tf_op jit(solution)/shard_map/all_to_all | solution.py:12
  348.3 30.5 %all_to_all.57 = bf16[8,384,256]{2,1,0:T(8,128)(2,1)S(1)} all-to-all(bf16[8,384,256]{2,1,0:T(8,128)(2,1)S(1)} %bitcast.128), channel_id=1, replica_groups=mesh['grp'=2,'fs'=16,'tp_0'=4,'tp_1'=2] {'tp_0','tp_1'}, dimensions={0} | all-to-all | bytes 3145728 | tf_op jit(solution)/shard_map/all_to_all | solution.py:44
  381.7 13.9 %all_to_all.58 = bf16[4,385,256]{2,1,0:T(8,128)(2,1)S(1)} all-to-all(bf16[4,385,256]{2,1,0:T(8,128)(2,1)S(1)} %broadcast_in_dim.105), channel_id=1, replica_groups=mesh['grp'=2,'fs'=16,'tp_0'=4,'tp_1'=2] {'tp_0'}, dimensions={0} | all-to-all | bytes 1576960 | tf_op jit(solution)/shard_map/all_to_all | solution.py:12
  396.3 6.5 %all_to_all.59 = bf16[2,4,385,256]{3,1,2,0:T(4,128)(2,1)S(1)} all-to-all(bf16[2,4,385,256]{3,1,2,0:T(4,128)(2,1)S(1)} %broadcast_in_dim.106), channel_id=1, replica_groups=mesh['grp'=2,'fs'=16,'tp_0'=4,'tp_1'=2] {'tp_1'}, dimensions={0} | all-to-all | bytes 3153920 | tf_op jit(solution)/shard_map/all_to_all | solution.py:12
  405.4 2.4 copy.49
  409.3 3.3 fusion.14
  412.6 6.5 %convolution_convert_fusion = bf16[384,2048]{1,0:T(8,128)(2,1)S(1)} fusion(bf16[768,2048]{0,1:T(8,128)(2,1)} %bitcast.7, bf16[384,2048]{0,1:T(8,128)(2,1)} %copy-done.2, bf16[2048,1536]{1,0:T(8,128)(2,1)} %all-gather.3.cloned.1.call-done, f32[384,768]{1,0:T(8,128)S(1)} %fusion.14, f32[384]{0:T(512)S(1)} %add_rsqrt_fusion), kind=kOutput, calls=%fused_computation.12 | convolution fusion | flops 2418769920 | bytes 10618368 | tf_op jit(solution)/shard_map/dot_general | solution.py:104
  419.2 23.4 %all_to_all.60 = bf16[8,384,256]{2,1,0:T(8,128)(2,1)S(1)} all-to-all(bf16[8,384,256]{2,1,0:T(8,128)(2,1)S(1)} %bitcast.129), channel_id=1, replica_groups=mesh['grp'=2,'fs'=16,'tp_0'=4,'tp_1'=2] {'tp_0','tp_1'}, dimensions={0} | all-to-all | bytes 3145728 | tf_op jit(solution)/shard_map/all_to_all | solution.py:44
  (95 shorter events, 35.2 us)
Async XLA Ops:
  6.5 339.3 %copy-start = (bf16[1,128,128]{2,1,0:T(8,128)(2,1)S(1)}, bf16[1,128,128]{2,1,0:T(8,128)(2,1)}, u32[]{:S(2)}) copy-start(bf16[1,128,128]{2,1,0:T(8,128)(2,1)} %param.20) | copy-start | bytes 98308
  6.6 7.2 %copy-start.9 = (bf16[128,768]{1,0:T(8,128)(2,1)S(1)}, bf16[128,768]{1,0:T(8,128)(2,1)}, u32[]{:S(2)}) copy-start(bf16[128,768]{1,0:T(8,128)(2,1)} %param.14) | copy-start | bytes 589828
  6.6 7.2 %copy-start.8 = (bf16[128,768]{1,0:T(8,128)(2,1)S(1)}, bf16[128,768]{1,0:T(8,128)(2,1)}, u32[]{:S(2)}) copy-start(bf16[128,768]{1,0:T(8,128)(2,1)} %param.15) | copy-start | bytes 589828
  8.5 6.1 %copy-start.7 = (bf16[768,128]{1,0:T(8,128)(2,1)S(1)}, bf16[768,128]{1,0:T(8,128)(2,1)}, u32[]{:S(2)}) copy-start(bf16[768,128]{1,0:T(8,128)(2,1)} %param.16) | copy-start | bytes 589828
  8.5 13.7 %all-to-all-start = ((bf16[4,385,256]{2,1,0:T(8,128)(2,1)}), bf16[4,385,256]{2,1,0:T(8,128)(2,1)S(1)}, u32[]{:S(2)}, u32[]{:S(2)}) async-start(bf16[4,385,256]{2,1,0:T(8,128)(2,1)} %broadcast_in_dim.91), calls=%async_computation | async-start | bytes 1605632 | tf_op jit(solution)/shard_map/all_to_all | solution.py:12
  13.8 233.3 %all-gather.3.cloned.1.call-start = ((), (), s32[]{:S(2)}) async-start(), calls=%async_computation.11 | async-start | bytes 6684672 | tf_op jit(solution)/shard_map/all_gather | solution.py:54
  49.5 202.0 %all-to-all-start.2 = ((bf16[16,768,128]{1,2,0:T(8,128)(2,1)}), bf16[16,768,128]{1,2,0:T(8,128)(2,1)}, u32[]{:S(2)}, u32[]{:S(2)}) async-start(bf16[16,768,128]{1,2,0:T(8,128)(2,1)} %stack.2), calls=%async_computation.2 | async-start | bytes 6291456 | tf_op jit(solution)/shard_map/all_to_all | solution.py:96
  259.1 7.8 %copy-start.10 = (bf16[128,256]{1,0:T(8,128)(2,1)S(1)}, bf16[128,256]{1,0:T(8,128)(2,1)}, u32[]{:S(2)}) copy-start(bf16[128,256]{1,0:T(8,128)(2,1)} %param.19) | copy-start | bytes 196612
  259.1 7.8 %copy-start.12 = (bf16[128,128]{1,0:T(8,128)(2,1)S(1)}, bf16[128,128]{1,0:T(8,128)(2,1)}, u32[]{:S(2)}) copy-start(bf16[128,128]{1,0:T(8,128)(2,1)} %param.18) | copy-start | bytes 98308
  259.1 28.3 %all-to-all-start.3 = ((bf16[8,384,256]{2,1,0:T(8,128)(2,1)}), bf16[8,384,256]{2,1,0:T(8,128)(2,1)S(1)}, u32[]{:S(2)}, u32[]{:S(2)}) async-start(bf16[8,384,256]{2,1,0:T(8,128)(2,1)} %bitcast.114), calls=%async_computation.3 | async-start | bytes 3145728 | tf_op jit(solution)/shard_map/all_to_all | solution.py:44
  266.9 20.8 %copy-start.3 = (bf16[384,256]{1,0:T(8,128)(2,1)S(1)}, bf16[384,256]{1,0:T(8,128)(2,1)}, u32[]{:S(2)}) copy-start(bf16[384,256]{1,0:T(8,128)(2,1)} %param.12) | copy-start | bytes 589828
  266.9 20.9 %copy-start.13 = (bf16[1,256]{1,0:T(2,128)(2,1)S(1)}, bf16[1,256]{1,0:T(2,128)(2,1)}, u32[]{:S(2)}) copy-start(bf16[1,256]{1,0:T(2,128)(2,1)} %param.17) | copy-start | bytes 1540
  266.9 64.8 %all-gather.5.cloned.1.call-start = ((), (), s32[]{:S(2)}) async-start(), calls=%async_computation.12 | async-start | bytes 1671168 | tf_op jit(solution)/shard_map/all_gather | solution.py:54
  287.8 4.6 %copy-start.11 = (bf16[128,128]{1,0:T(8,128)(2,1)S(1)}, bf16[128,128]{1,0:T(8,128)(2,1)}, u32[]{:S(2)}) copy-start(bf16[128,128]{1,0:T(8,128)(2,1)} %param.22) | copy-start | bytes 98308
  288.7 15.1 %all-to-all-start.4 = ((bf16[4,385,256]{2,1,0:T(8,128)(2,1)}), bf16[4,385,256]{2,1,0:T(8,128)(2,1)S(1)}, u32[]{:S(2)}, u32[]{:S(2)}) async-start(bf16[4,385,256]{2,1,0:T(8,128)(2,1)} %broadcast_in_dim.93), calls=%async_computation.4 | async-start | bytes 1605632 | tf_op jit(solution)/shard_map/all_to_all | solution.py:12
  312.0 33.9 %all-to-all-start.6 = ((bf16[16,128,128]{1,2,0:T(8,128)(2,1)}), bf16[16,128,128]{1,2,0:T(8,128)(2,1)}, u32[]{:S(2)}, u32[]{:S(2)}) async-start(bf16[16,128,128]{1,2,0:T(8,128)(2,1)} %broadcast_in_dim.104), calls=%async_computation.6 | async-start | bytes 1048576 | tf_op jit(solution)/shard_map/all_to_all | solution.py:12
  333.4 0.7 copy-start.6
  333.4 12.4 %copy-start.16 = (f32[1,128]{1,0:T(1,128)S(1)}, f32[1,128]{1,0:T(1,128)}, u32[]{:S(2)}) copy-start(f32[1,128]{1,0:T(1,128)} %param.21) | copy-start | bytes 1540
  378.8 1.4 copy-start.15
  380.2 0.7 copy-start.14
  380.9 0.7 copy-start.4
  408.1 1.1 copy-start.2
  419.2 25.1 %copy-start.1 = (bf16[1,128,128]{2,1,0:T(8,128)(2,1)S(1)}, bf16[1,128,128]{2,1,0:T(8,128)(2,1)}, u32[]{:S(2)}) copy-start(bf16[1,128,128]{2,1,0:T(8,128)(2,1)} %param.20) | copy-start | bytes 98308
  442.7 0.9 copy-start.5
Sparse Core Ops, SparseCore 0:
  16.4 230.6 all-gather.2
  269.5 62.1 all-gather.4
